TPU v7x, 32 devices: a whole 2x2x4 slice. The times are simulated.
32 devices in a mesh: rep: 2 (over y), fs: 4 (over z), tp: 4 (over x, core).
Axes of the slice: x: 2, y: 2, z: 4, core: 2. Of those that a mesh axis runs over, the one named last changes fastest.
Arguments:
- gate_pre: bfloat16 [8192, 3072], P(('rep', 'fs'), 'tp'), may hold values from -6 to 6
- up_pre: bfloat16 [8192, 3072], P(('rep', 'fs'), 'tp'), may hold values from -6 to 6
- out_grad: bfloat16 [8192, 2048], P(('rep', 'fs')), may hold values from -8 to 8
- w_down: bfloat16 [3072, 2048], P('tp', 'fs'), may hold values from -0.109375 to 0.109375
Outputs:
- d_gate: bfloat16 [8192, 3072], P(('rep', 'fs'), 'tp')
- d_up: bfloat16 [8192, 3072], P(('rep', 'fs'), 'tp')
- grad_down: float32 [3072, 2048], P('tp', 'fs')
- row_energy: float32 [3072], P('tp')
All inputs are finite; a program needn't handle non-finite values.
Results may differ from a plain program's by a relative error of at most 0.0034.
Values may be sent and summed in bfloat16 or wider, within the bound.
A program may use at most 64 MiB of HBM per device.

v0:
```python
import jax
import jax.numpy as jnp
from jax import lax
from jax.sharding import PartitionSpec as P

D = 2048


def local(gate_pre, up_pre, out_grad, w_down):
    gate_f = gate_pre.astype(jnp.float32)
    up_f = up_pre.astype(jnp.float32)
    sig = jax.nn.sigmoid(gate_f)
    act = gate_f * sig
    hidden = (act * up_f).astype(jnp.bfloat16)
    tokens_all = out_grad.shape[0] * lax.axis_size("rep") * lax.axis_size("fs")
    factor = float(tokens_all) ** (-0.5)
    weight_whole = lax.all_gather(w_down, "fs", axis=1, tiled=True)
    dhid = lax.dot_general(
        out_grad, weight_whole, (((1,), (1,)), ((), ())), preferred_element_type=jnp.float32
    )
    d_up = (dhid * act).astype(jnp.bfloat16)
    d_gate = (dhid * up_f * sig * (1.0 + gate_f * (1.0 - sig))).astype(jnp.bfloat16)
    d_gate, d_up = (d_gate, d_up)
    shard = lax.psum_scatter(
        lax.dot_general(
            out_grad, hidden, (((0,), (0,)), ((), ())), preferred_element_type=jnp.float32
        ),
        "fs",
        scatter_dimension=0,
        tiled=True,
    )
    shard = lax.psum(shard, "rep")
    grad_down = shard.T * factor
    energy = lax.psum(jnp.sum(grad_down * grad_down, axis=1), "fs") / D
    return (d_gate, d_up, grad_down, energy)


def solution(mesh):
    placed = (P(("rep", "fs"), "tp"), P(("rep", "fs"), "tp"), P(("rep", "fs"), None), P("tp", "fs"))
    return jax.shard_map(
        local,
        mesh=mesh,
        in_specs=placed,
        out_specs=(P(("rep", "fs"), "tp"), P(("rep", "fs"), "tp"), P("tp", "fs"), P("tp")),
        check_vma=False,
    )
```

profile of v0, /device:TPU:0, one launch (start us, length us, event | category | flops | bytes accessed | tf_op | source)
XLA Modules:
  0.0 269.9 jit_solution(15199787096322260005)
XLA Ops:
  7.2 0.0 reduce-scatter.2.cloned.1.call-start
  7.2 9.4 %convolution_bitcast_fusion = f32[2048,768]{0,1:T(8,128)} fusion(bf16[1024,2048]{1,0:T(8,128)(2,1)} %param.6, bf16[1024,768]{1,0:T(8,128)(2,1)} %param.5, bf16[1024,768]{1,0:T(8,128)(2,1)} %param.4), kind=kOutput, calls=%fused_computation.5 | convolution fusion | flops 3227516928 | bytes 13631488 | tf_op jit(solution)/shard_map/dot_general | solution.py:25
  16.6 0.0 copy-start
  16.7 0.0 copy-start.1
  16.7 0.0 reduce-scatter.2.cloned.1.call-update
  16.7 0.0 all-gather.2.cloned.1.call-start
  16.7 0.7 all-gather.2.cloned.1.call-update
  17.4 0.0 all-reduce.2.cloned.1.call-start
  17.5 112.9 %reduce-scatter.2.cloned.1.call-done = f32[512,768]{0,1:T(8,128)} async-done(((f32[2048,768]{0,1:T(8,128)}), f32[512,768]{0,1:T(8,128)}) %reduce-scatter.2.cloned.1.call-update) | async-done | bytes 1572880 | tf_op jit(solution)/shard_map/reduce_scatter | solution.py:24
  130.4 0.0 all-reduce.2.cloned.1.call-update
  130.4 65.5 %all-gather.2.cloned.1.call-done = bf16[768,2048]{1,0:T(8,128)(2,1)} async-done(((bf16[768,512]{1,0:T(8,128)(2,1)}), bf16[768,2048]{1,0:T(8,128)(2,1)}) %all-gather.2.cloned.1.call-update) | async-done | bytes 3145744 | tf_op jit(solution)/shard_map/all_gather | solution.py:17
  195.9 0.0 copy-done
  195.9 0.0 copy-done.1
  195.9 9.2 %multiply_convert_fusion = (bf16[1024,768]{1,0:T(8,128)(2,1)}, bf16[1024,768]{1,0:T(8,128)(2,1)}) fusion(bf16[1024,768]{1,0:T(8,128)(2,1)S(1)} %copy-done, bf16[1024,768]{1,0:T(8,128)(2,1)S(1)} %copy-done.1, bf16[1024,2048]{1,0:T(8,128)(2,1)} %param.6, bf16[768,2048]{1,0:T(8,128)(2,1)} %all-gather.2.cloned.1.call-done), kind=kOutput, calls=%fused_computation.14 | convolution fusion | flops 3233021952 | bytes 13631488 | tf_op jit(solution)/shard_map/dot_general | solution.py:18
  205.0 43.4 %all-reduce.2.cloned.1.call-done = f32[512,768]{0,1:T(8,128)} async-done(((f32[512,768]{0,1:T(8,128)}), f32[512,768]{0,1:T(8,128)}) %all-reduce.2.cloned.1.call-update) | async-done | bytes 1572880 | tf_op jit(solution)/shard_map/psum | solution.py:32
  248.4 2.7 multiply_reduce_fusion
  251.1 11.7 %psum.15 = f32[768]{0:T(1024)S(1)} all-reduce(f32[768]{0:T(1024)S(1)} %get-tuple-element.4), channel_id=1, replica_groups=mesh['rep'=2,'fs'=4,'tp'=4] {'fs'}, use_global_device_ids=true, to_apply=%region_3.0 | all-reduce | flops 768 | bytes 6144 | tf_op jit(solution)/shard_map/psum | solution.py:34
  262.8 0.6 broadcast_multiply_fusion
Async XLA Ops:
  7.2 123.2 %reduce-scatter.2.cloned.1.call-start = ((), (), s32[]{:S(2)}) async-start(), calls=%async_computation.2 | async-start | bytes 7864320 | tf_op jit(solution)/shard_map/reduce_scatter | solution.py:24
  16.6 179.2 %copy-start = (bf16[1024,768]{1,0:T(8,128)(2,1)S(1)}, bf16[1024,768]{1,0:T(8,128)(2,1)}, u32[]{:S(2)}) copy-start(bf16[1024,768]{1,0:T(8,128)(2,1)} %param.4) | copy-start | bytes 4718596
  16.7 179.2 %copy-start.1 = (bf16[1024,768]{1,0:T(8,128)(2,1)S(1)}, bf16[1024,768]{1,0:T(8,128)(2,1)}, u32[]{:S(2)}) copy-start(bf16[1024,768]{1,0:T(8,128)(2,1)} %param.5) | copy-start | bytes 4718596
  16.7 179.2 %all-gather.2.cloned.1.call-start = ((), (), s32[]{:S(2)}) async-start(), calls=%async_computation.1 | async-start | bytes 3932160 | tf_op jit(solution)/shard_map/all_gather | solution.py:17
  17.4 231.0 %all-reduce.2.cloned.1.call-start = ((), (), s32[]{:S(2)}) async-start(), calls=%async_computation.3 | async-start | bytes 3145728 | tf_op jit(solution)/shard_map/psum | solution.py:32
Sparse Core Ops, SparseCore 0:
  16.8 113.5 reduce-scatter.1
  131.9 63.9 all-gather.1
  198.2 50.1 all-reduce.1
where the time goes:
time: 270 us
  waiting for transfers between devices  222 us (82%)
  matrix products  18.6 us (7%)
  between operations  13.7 us (5%)
  blocking collectives  11.7 us (4%)
  other arithmetic  3.29 us (1%)
    reduce_scatter x1, waiting for transfers between devices, local(): lax.psum_scatter(lax.dot_general(out_grad, hidden, (((0,), (0,)), ((), ()...  113 us
    all_gather x1, waiting for transfers between devices, local(): weight_whole = lax.all_gather(w_down, 'fs', axis=1, tiled=True)  65.5 us
    psum x1, waiting for transfers between devices, local(): shard = lax.psum(shard, 'rep')  43.4 us
    psum x1, blocking collectives, local(): energy = lax.psum(jnp.sum(grad_down * grad_down, axis=1), 'fs') / D  11.7 us
    dot_general x1, matrix products, local(): lax.dot_general(out_grad, hidden, (((0,), (0,)), ((), ())), preferred_ele...  9.44 us
    dot_general x1, matrix products, local(): lax.dot_general(out_grad, weight_whole, (((1,), (1,)), ((), ())), preferr...  9.15 us
  transfers between devices with their start and end apart: 3, of which 3 were waited for; matrix products, arithmetic and copies ran while one was open for 3% of the time, Pallas kernels for 0%

commit v1 on v0

--- a/solution.py
+++ b/solution.py
@@ -14,7 +14,12 @@
     hidden = (act * up_f).astype(jnp.bfloat16)
     tokens_all = out_grad.shape[0] * lax.axis_size("rep") * lax.axis_size("fs")
     factor = float(tokens_all) ** (-0.5)
-    weight_whole = lax.all_gather(w_down, "fs", axis=1, tiled=True)
+    ring = [w_down]
+    for hop in range(3):
+        ring.append(lax.ppermute(ring[-1], "fs", [(dev, (dev + 1) % 4) for dev in range(4)]))
+    weight_whole = jnp.roll(
+        jnp.concatenate(ring[::-1], axis=1), (lax.axis_index("fs") + 1) * ring[0].shape[1], axis=1
+    )
     dhid = lax.dot_general(
         out_grad, weight_whole, (((1,), (1,)), ((), ())), preferred_element_type=jnp.float32
     )

time: 270 us -> 255 us (0.944)
  waiting for transfers between devices: 222 us -> 164 us
  starting transfers between devices: 0.12 us -> 29.3 us
  local copies, waits for them, and re-layouts: 0.01 us -> 15.6 us
    ppermute x0 -> x3, waiting for transfers between devices: none -> 106 us  [local(): lax.ppermute(ring[-1], 'fs', [(dev, (dev + 1) % 4) for dev in range(4)])]
    reduce_scatter x1, waiting for transfers between devices: 113 us -> 18.9 us  [local(): lax.psum_scatter(lax.dot_general(out_grad, hidden, (((0,), (0,)), ((), ()...]
    all_gather x1 -> x0, waiting for transfers between devices: 65.5 us -> none  [local(): weight_whole = lax.all_gather(w_down, 'fs', axis=1, tiled=True)]
    ppermute x0 -> x3, starting transfers between devices: none -> 29.2 us  [local(): lax.ppermute(ring[-1], 'fs', [(dev, (dev + 1) % 4) for dev in range(4)])]
    unnamed x4 -> x21, local copies, waits for them, and re-layouts: 0.01 us -> 14.6 us
    psum x1, waiting for transfers between devices: 43.4 us -> 39.4 us  [local(): shard = lax.psum(shard, 'rep')]
  transfers between devices with their start and end apart: 3 -> 5, of which waited for: 3 -> 5; matrix products, arithmetic and copies ran while one was open for 3% -> 7% of each run, Pallas kernels for 0% -> 0%
where the time goes in v1:
time: 255 us
  waiting for transfers between devices  164 us (64%)
  starting transfers between devices  29.3 us (11%)
  matrix products  16.6 us (7%)
  local copies, waits for them, and re-layouts  15.6 us (6%)
  between operations  14.1 us (6%)
  blocking collectives  11.7 us (5%)
  other arithmetic  3.29 us (1%)
    ppermute x3, waiting for transfers between devices, local(): lax.ppermute(ring[-1], 'fs', [(dev, (dev + 1) % 4) for dev in range(4)])  106 us
    psum x1, waiting for transfers between devices, local(): shard = lax.psum(shard, 'rep')  39.4 us
    ppermute x3, starting transfers between devices, local(): lax.ppermute(ring[-1], 'fs', [(dev, (dev + 1) % 4) for dev in range(4)])  29.2 us
    reduce_scatter x1, waiting for transfers between devices, local(): lax.psum_scatter(lax.dot_general(out_grad, hidden, (((0,), (0,)), ((), ()...  18.9 us
    unnamed x21, local copies, waits for them, and re-layouts  14.6 us
    psum x1, blocking collectives, local(): energy = lax.psum(jnp.sum(grad_down * grad_down, axis=1), 'fs') / D  11.7 us
    dot_general x1, matrix products, local(): lax.dot_general(out_grad, hidden, (((0,), (0,)), ((), ())), preferred_ele...  8.95 us
    dot_general x1, matrix products, local(): lax.dot_general(out_grad, weight_whole, (((1,), (1,)), ((), ())), preferr...  7.65 us
  transfers between devices with their start and end apart: 5, of which 5 were waited for; matrix products, arithmetic and copies ran while one was open for 7% of the time, Pallas kernels for 0%

profile of v1, /device:TPU:0, one launch (start us, length us, event | category | flops | bytes accessed | tf_op | source)
XLA Modules:
  0.0 255.0 jit_solution(8566976605577621541)
XLA Ops:
  7.2 0.0 copy-start.1
  7.2 0.0 reduce-scatter.2.cloned.1.call-start
  7.2 1.8 copy.8
  9.1 0.0 copy-done.1
  9.1 0.0 copy-start.2
  9.1 1.6 copy.9
  10.7 9.0 %convolution_bitcast_fusion = f32[2048,768]{0,1:T(8,128)} fusion(bf16[1024,2048]{1,0:T(8,128)(2,1)} %param.6, bf16[1024,768]{0,1:T(8,128)(2,1)S(1)} %copy.8, bf16[1024,768]{0,1:T(8,128)(2,1)} %copy.9), kind=kOutput, calls=%fused_computation.5 | convolution fusion | flops 3227516928 | bytes 13631488 | tf_op jit(solution)/shard_map/dot_general | solution.py:30
  19.7 0.0 copy-done.2
  19.7 0.0 copy-start
  19.7 0.0 reduce-scatter.2.cloned.1.call-update
  19.7 0.0 all-reduce.2.cloned.1.call-start
  19.8 1.1 copy-done
  20.8 3.1 %collective-permute-start = (bf16[768,512]{1,0:T(8,128)(2,1)S(1)}, bf16[768,512]{1,0:T(8,128)(2,1)S(1)}, u32[]{:S(2)}, u32[]{:S(2)}) collective-permute-start(bf16[768,512]{1,0:T(8,128)(2,1)S(1)} %copy-done), channel_id=1, source_target_pairs={{0,4},{4,8},{8,12},{12,0},{1,5},{5,9},{9,13},{13,1},{2,6},{6,10},{... | collective-permute-start | bytes 2359304 | tf_op jit(solution)/shard_map/ppermute | solution.py:19
  23.9 31.5 %collective-permute-done = bf16[768,512]{1,0:T(8,128)(2,1)S(1)} collective-permute-done((bf16[768,512]{1,0:T(8,128)(2,1)S(1)}, bf16[768,512]{1,0:T(8,128)(2,1)S(1)}, u32[]{:S(2)}, u32[]{:S(2)}) %collective-permute-start) | collective-permute-done | bytes 786464 | tf_op jit(solution)/shard_map/ppermute | solution.py:19
  55.3 8.5 %collective-permute-start.1 = (bf16[768,512]{1,0:T(8,128)(2,1)S(1)}, bf16[768,512]{1,0:T(8,128)(2,1)S(1)}, u32[]{:S(2)}, u32[]{:S(2)}) collective-permute-start(bf16[768,512]{1,0:T(8,128)(2,1)S(1)} %collective-permute-done), channel_id=1, source_target_pairs={{0,4},{4,8},{8,12},{12,0},{1,5},{5,9},{9,13},{13,1},{2,6},{6,10},{... | collective-permute-start | bytes 2359304 | tf_op jit(solution)/shard_map/ppermute | solution.py:19
  63.9 38.1 %collective-permute-done.1 = bf16[768,512]{1,0:T(8,128)(2,1)S(1)} collective-permute-done((bf16[768,512]{1,0:T(8,128)(2,1)S(1)}, bf16[768,512]{1,0:T(8,128)(2,1)S(1)}, u32[]{:S(2)}, u32[]{:S(2)}) %collective-permute-start.1) | collective-permute-done | bytes 786464 | tf_op jit(solution)/shard_map/ppermute | solution.py:19
  101.9 17.6 %collective-permute-start.2 = (bf16[768,512]{1,0:T(8,128)(2,1)S(1)}, bf16[768,512]{1,0:T(8,128)(2,1)S(1)}, u32[]{:S(2)}, u32[]{:S(2)}) collective-permute-start(bf16[768,512]{1,0:T(8,128)(2,1)S(1)} %collective-permute-done.1), channel_id=1, source_target_pairs={{0,4},{4,8},{8,12},{12,0},{1,5},{5,9},{9,13},{13,1},{2,6},{6,10},{... | collective-permute-start | bytes 2359304 | tf_op jit(solution)/shard_map/ppermute | solution.py:19
  119.6 36.6 %collective-permute-done.2 = bf16[768,512]{1,0:T(8,128)(2,1)S(1)} collective-permute-done((bf16[768,512]{1,0:T(8,128)(2,1)S(1)}, bf16[768,512]{1,0:T(8,128)(2,1)S(1)}, u32[]{:S(2)}, u32[]{:S(2)}) %collective-permute-start.2) | collective-permute-done | bytes 786464 | tf_op jit(solution)/shard_map/ppermute | solution.py:19
  156.1 1.0 constant_dynamic-update-slice_fusion.7
  157.1 1.0 constant_dynamic-update-slice_fusion.6
  158.1 1.0 constant_dynamic-update-slice_fusion.5
  159.1 0.9 constant_dynamic-update-slice_fusion.4
  160.0 1.0 constant_dynamic-update-slice_fusion.3
  161.0 18.9 %reduce-scatter.2.cloned.1.call-done = f32[512,768]{0,1:T(8,128)} async-done(((f32[2048,768]{0,1:T(8,128)}), f32[512,768]{0,1:T(8,128)}) %reduce-scatter.2.cloned.1.call-update) | async-done | bytes 1572880 | tf_op jit(solution)/shard_map/reduce_scatter | solution.py:29
  180.0 0.0 all-reduce.2.cloned.1.call-update
  180.0 0.0 copy-start.3
  180.0 0.0 copy-start.4
  180.0 1.0 constant_dynamic-update-slice_fusion.2
  181.0 1.0 constant_dynamic-update-slice_fusion.1
  182.0 1.0 constant_dynamic-update-slice_fusion
  183.0 0.0 copy-done.3
  183.0 0.0 copy-done.4
  183.0 7.7 %fusion.8 = (bf16[1024,768]{0,1:T(8,128)(2,1)S(1)}, bf16[1024,768]{0,1:T(8,128)(2,1)S(1)}) fusion(bf16[1024,768]{0,1:T(8,128)(2,1)S(1)} %copy-done.4, bf16[1024,768]{0,1:T(8,128)(2,1)S(1)} %copy-done.3, bf16[1024,2048]{1,0:T(8,128)(2,1)} %param.6, bf16[768,4096]{1,0:T(8,128)(2,1)} %constant_dynamic-update-slice_fusion, s32[]{:T(128)S(6)} %select_n.14), kind=kOutput, calls=%fused_computation.15 | convolution fusion | flops 3233021952 | bytes 13631492 | tf_op jit(solution)/shard_map/dot_general | solution.py:23
  190.7 1.6 copy.10
  192.2 1.6 copy.11
  193.8 39.4 %all-reduce.2.cloned.1.call-done = f32[512,768]{0,1:T(8,128)} async-done(((f32[512,768]{0,1:T(8,128)}), f32[512,768]{0,1:T(8,128)}) %all-reduce.2.cloned.1.call-update) | async-done | bytes 1572880 | tf_op jit(solution)/shard_map/psum | solution.py:37
  233.2 2.7 %multiply_reduce_fusion = (f32[768]{0:T(1024)S(1)}, f32[768,512]{1,0:T(8,128)}) fusion(f32[512,768]{0,1:T(8,128)} %all-reduce.2.cloned.1.call-done), kind=kLoop, calls=%fused_computation.18 | loop fusion | flops 1178880 | bytes 3148800 | tf_op jit(solution)/shard_map/reduce_sum | solution.py:39
  235.9 11.7 %psum.15 = f32[768]{0:T(1024)S(1)} all-reduce(f32[768]{0:T(1024)S(1)} %get-tuple-element.8), channel_id=1, replica_groups=mesh['rep'=2,'fs'=4,'tp'=4] {'fs'}, use_global_device_ids=true, to_apply=%region_3.4 | all-reduce | flops 768 | bytes 6144 | tf_op jit(solution)/shard_map/psum | solution.py:39
  247.6 0.6 broadcast_multiply_fusion
Async XLA Ops:
  7.2 1.9 copy-start.1
  7.2 172.8 %reduce-scatter.2.cloned.1.call-start = ((), (), s32[]{:S(2)}) async-start(), calls=%async_computation.1 | async-start | bytes 7864320 | tf_op jit(solution)/shard_map/reduce_scatter | solution.py:29
  9.1 10.6 %copy-start.2 = (bf16[1024,768]{0,1:T(8,128)(2,1)}, bf16[1024,768]{0,1:T(8,128)(2,1)S(1)}, u32[]{:S(2)}) copy-start(bf16[1024,768]{0,1:T(8,128)(2,1)S(1)} %copy.8) | copy-start | bytes 4718596
  19.7 1.1 copy-start
  19.7 213.5 %all-reduce.2.cloned.1.call-start = ((), (), s32[]{:S(2)}) async-start(), calls=%async_computation.2 | async-start | bytes 3145728 | tf_op jit(solution)/shard_map/psum | solution.py:37
  20.8 34.5 %collective-permute-start = (bf16[768,512]{1,0:T(8,128)(2,1)S(1)}, bf16[768,512]{1,0:T(8,128)(2,1)S(1)}, u32[]{:S(2)}, u32[]{:S(2)}) collective-permute-start(bf16[768,512]{1,0:T(8,128)(2,1)S(1)} %copy-done), channel_id=1, source_target_pairs={{0,4},{4,8},{8,12},{12,0},{1,5},{5,9},{9,13},{13,1},{2,6},{6,10},{... | collective-permute-start | bytes 2359304 | tf_op jit(solution)/shard_map/ppermute | solution.py:19
  55.3 46.6 %collective-permute-start.1 = (bf16[768,512]{1,0:T(8,128)(2,1)S(1)}, bf16[768,512]{1,0:T(8,128)(2,1)S(1)}, u32[]{:S(2)}, u32[]{:S(2)}) collective-permute-start(bf16[768,512]{1,0:T(8,128)(2,1)S(1)} %collective-permute-done), channel_id=1, source_target_pairs={{0,4},{4,8},{8,12},{12,0},{1,5},{5,9},{9,13},{13,1},{2,6},{6,10},{... | collective-permute-start | bytes 2359304 | tf_op jit(solution)/shard_map/ppermute | solution.py:19
  101.9 54.2 %collective-permute-start.2 = (bf16[768,512]{1,0:T(8,128)(2,1)S(1)}, bf16[768,512]{1,0:T(8,128)(2,1)S(1)}, u32[]{:S(2)}, u32[]{:S(2)}) collective-permute-start(bf16[768,512]{1,0:T(8,128)(2,1)S(1)} %collective-permute-done.1), channel_id=1, source_target_pairs={{0,4},{4,8},{8,12},{12,0},{1,5},{5,9},{9,13},{13,1},{2,6},{6,10},{... | collective-permute-start | bytes 2359304 | tf_op jit(solution)/shard_map/ppermute | solution.py:19
  180.0 3.0 %copy-start.3 = (bf16[1024,768]{0,1:T(8,128)(2,1)S(1)}, bf16[1024,768]{0,1:T(8,128)(2,1)}, u32[]{:S(2)}) copy-start(bf16[1024,768]{0,1:T(8,128)(2,1)} %copy-done.2) | copy-start | bytes 4718596
  180.0 3.0 %copy-start.4 = (bf16[1024,768]{0,1:T(8,128)(2,1)S(1)}, bf16[1024,768]{0,1:T(8,128)(2,1)}, u32[]{:S(2)}) copy-start(bf16[1024,768]{0,1:T(8,128)(2,1)} %copy.9) | copy-start | bytes 4718596
Sparse Core Ops, SparseCore 0:
  19.8 160.0 reduce-scatter.1
  182.3 50.9 all-reduce.1
